TPU v7x, 32 devices: a whole 2x2x4 slice. The times are simulated.
32 devices in a mesh: ep: 8 (over z, x), tp: 4 (over y, core).
Axes of the slice: x: 2, y: 2, z: 4, core: 2. Of those that a mesh axis runs over, the one named last changes fastest.
Arguments:
- mixer_in: bfloat16 [1024, 2048], P('ep'), may hold values from -6 to 6
- mixer_gain: float32 [2048], replicated, may hold values from 0.1 to 1.9
- w_value: bfloat16 [2048, 1536], P(None, 'tp'), may hold values from -0.125 to 0.125
- w_gate: bfloat16 [2048, 1536], P(None, 'tp'), may hold values from -0.125 to 0.125
- w_taps: float32 [31, 1536], P(None, 'tp'), may hold values from -3 to 3
- channel_gain: float32 [1536], P('tp'), may hold values from 0.1 to 1.9
- w_output: bfloat16 [1536, 2048], P('tp'), may hold values from -0.15625 to 0.15625
- expert_in: bfloat16 [1024, 2048], P('ep'), may hold values from -6 to 6
- expert_gain: float32 [2048], replicated, may hold values from 0 to 8
- route_experts: int32 [1024, 4], P('ep'), may hold values from 0 to 7, all different within a row; in each aligned block of 128 rows (0 to 127, 128 to 255, ...) at most 128 rows name the same one
- route_scores: float32 [1024, 4], P('ep'), may hold values from -6 to 6
- expert_gate: bfloat16 [8, 2048, 2048], P('ep', None, 'tp'), may hold values from -0.125 to 0.125
- expert_up: bfloat16 [8, 2048, 2048], P('ep', None, 'tp'), may hold values from -0.125 to 0.125
- expert_down: bfloat16 [8, 2048, 2048], P('ep', 'tp'), may hold values from -0.125 to 0.125
Outputs:
- mixer_out: bfloat16 [1024, 2048], P('ep')
- expert_out: bfloat16 [1024, 2048], P('ep')
Inputs may be any that keep to these rules, and one draw needn't show every extreme that they name: `route_experts`: each row names 4 different experts. In each aligned block of 128 rows (the rows of one index of ep) no expert is named more than 128 times, a bound that some block reaches.
All inputs are finite; a program needn't handle non-finite values.
Results may differ from a plain program's by a relative error of at most 0.02.
Values may be sent and summed in bfloat16 or wider, within the bound.
A program may use at most 64 MiB of HBM per device.

v0:
```python
import jax
import jax.numpy as jnp
from jax import lax
from jax.sharding import PartitionSpec as P

CONV_CH = 1536
CONV_W = 31
TOP_K = 4
epsilon = 1e-05
clamp_limit = 7.0
swish_slope = 1.702


def shifted(block, axis, distance):
    devices = range(lax.axis_size(axis))
    route = [(i - distance, i) for i in devices if i - distance in devices]
    return lax.ppermute(block, axis, route)


def row_norm(inputs, gains):
    widened = inputs.astype(jnp.float32)
    row_mean = jnp.mean(widened, axis=-1, keepdims=True)
    row_var = jnp.mean(jnp.square(widened - row_mean), axis=-1, keepdims=True)
    return (widened - row_mean) * lax.rsqrt(row_var + epsilon) * gains


def local(
    mixer_in,
    mixer_gain,
    w_value,
    w_gate,
    w_taps,
    channel_gain,
    w_output,
    expert_in,
    expert_gain,
    route_experts,
    route_scores,
    expert_gate,
    expert_up,
    expert_down,
):
    normed = row_norm(mixer_in, mixer_gain).astype(jnp.bfloat16)
    values = jnp.dot(normed, w_value, preferred_element_type=jnp.float32)
    gate_pre = jnp.dot(normed, w_gate, preferred_element_type=jnp.float32)
    gated_values = (values * jax.nn.sigmoid(gate_pre)).astype(jnp.bfloat16)
    mixer_rows = gated_values.shape[0]
    reach_rows = CONV_W - 1
    earlier = shifted(gated_values[mixer_rows - reach_rows :], "ep", 1)
    extended = jnp.concatenate([earlier, gated_values], axis=0)
    conv_out = jnp.zeros(gated_values.shape, jnp.float32)
    for offset in range(CONV_W):
        conv_out = (
            conv_out + extended[offset : offset + mixer_rows].astype(jnp.float32) * w_taps[offset]
        )
    channel_sums = lax.psum(
        (
            jnp.sum(conv_out, axis=1, keepdims=True),
            jnp.sum(conv_out * conv_out, axis=1, keepdims=True),
        ),
        "tp",
    )
    row_mean = channel_sums[0] / CONV_CH
    row_var = channel_sums[1] / CONV_CH - row_mean * row_mean
    activated = jax.nn.silu(
        (conv_out - row_mean) * lax.rsqrt(row_var + epsilon) * channel_gain
    ).astype(jnp.bfloat16)
    mixer_out = lax.psum(
        jnp.dot(activated, w_output, preferred_element_type=jnp.float32).astype(jnp.bfloat16), "tp"
    )
    rows_b = expert_in.shape[0]
    width = expert_in.shape[1]
    experts = lax.axis_size("ep")
    capacity = 2 * rows_b * TOP_K // experts
    slot_share = capacity // lax.axis_size("tp")
    column = lax.axis_index("tp")
    normed_b = row_norm(expert_in, expert_gain).astype(jnp.bfloat16)
    raised = jnp.exp(route_scores)
    route_weights = raised / jnp.sum(raised, axis=1, keepdims=True)
    flat_ids = route_experts.reshape(-1)
    onehot = (flat_ids[:, None] == jnp.arange(experts, dtype=jnp.int32)[None, :]).astype(jnp.int32)
    slot_index = jnp.sum((jnp.cumsum(onehot, axis=0) - onehot) * onehot, axis=1)
    owner_row = jnp.arange(rows_b * TOP_K, dtype=jnp.int32) // TOP_K
    slot_table = (
        jnp.full((capacity * experts,), rows_b, jnp.int32)
        .at[slot_index * experts + flat_ids]
        .set(owner_row)
    )
    padded = jnp.concatenate([normed_b, jnp.zeros((1, width), jnp.bfloat16)], axis=0)
    gate_w = expert_gate[0]
    up_w = expert_up[0]
    down_w = expert_down[0]
    own_table = lax.dynamic_slice_in_dim(
        slot_table, column * slot_share * experts, slot_share * experts
    )
    sending = jnp.take(padded, own_table, axis=0).reshape(slot_share, experts, width)
    arrived = lax.all_to_all(sending, "ep", split_axis=1, concat_axis=1, tiled=True)
    block_rows = lax.all_gather(arrived, "tp", axis=0, tiled=True)
    flat_rows = block_rows.reshape(block_rows.shape[0] * block_rows.shape[1], block_rows.shape[2])
    gate_e = jnp.minimum(
        jnp.dot(flat_rows, gate_w, preferred_element_type=jnp.float32), clamp_limit
    )
    up_e = jnp.clip(
        jnp.dot(flat_rows, up_w, preferred_element_type=jnp.float32), -clamp_limit, clamp_limit
    )
    hidden = (
        ((up_e + 1.0) * gate_e * jax.nn.sigmoid(swish_slope * gate_e))
        .astype(jnp.bfloat16)
        .reshape(block_rows.shape[0], block_rows.shape[1], gate_w.shape[1])
        .reshape(capacity * experts, gate_w.shape[1])
    )
    summed = lax.psum_scatter(
        jnp.dot(hidden, down_w, preferred_element_type=jnp.float32).astype(jnp.bfloat16),
        "tp",
        scatter_dimension=0,
        tiled=True,
    )
    returned = lax.all_to_all(
        summed.reshape(slot_share, experts, width), "ep", split_axis=1, concat_axis=1, tiled=True
    )
    every_slot = lax.all_gather(returned, "tp", axis=0, tiled=True).reshape(
        capacity * experts, width
    )
    picked = jnp.take(every_slot, slot_index * experts + flat_ids, axis=0)
    picked = picked.reshape(rows_b, TOP_K, width).astype(jnp.float32)
    expert_out = jnp.sum(picked * route_weights[:, :, None], axis=1).astype(jnp.bfloat16)
    return (mixer_out, expert_out)


def solution(mesh):
    in_specs = (
        P("ep", None),
        P(),
        P(None, "tp"),
        P(None, "tp"),
        P(None, "tp"),
        P("tp"),
        P("tp", None),
        P("ep", None),
        P(),
        P("ep", None),
        P("ep", None),
        P("ep", None, "tp"),
        P("ep", None, "tp"),
        P("ep", "tp", None),
    )
    out_specs = (P("ep", None), P("ep", None))
    return jax.shard_map(local, mesh=mesh, in_specs=in_specs, out_specs=out_specs, check_vma=False)
```

profile of v0, /device:TPU:0, one launch (start us, length us, event | category | flops | bytes accessed | tf_op | source)
XLA Modules:
  0.0 263.1 jit_solution(18099323295168561547)
XLA Ops:
  7.2 0.0 copy-start
  7.2 0.0 all-gather.3.cloned.1.call-start
  7.2 0.9 copy.33
  8.2 0.1 eq.29
  8.3 0.1 eq.25
  8.4 0.1 reshape.119
  8.5 1.1 reduce-window.6
  9.7 0.2 slice_reduce_fusion
  9.9 0.1 fusion.68
  10.0 2.4 scatter_custom_fusion
  12.5 0.1 compare_and_fusion
  12.6 1.2 convert_reduce_fusion
  13.8 1.3 fusion.24
  15.1 0.1 broadcast_in_dim.49
  15.2 0.1 copy.38
  15.3 1.4 fusion.26
  16.8 2.3 gather_fusion
  19.1 2.4 copy_select_fusion
  21.6 32.8 %all_to_all.10 = bf16[32,8,2048]{2,0,1:T(8,128)(2,1)S(1)} all-to-all(bf16[32,8,2048]{2,0,1:T(8,128)(2,1)S(1)} %copy_select_fusion), channel_id=1, replica_groups=mesh['ep'=8,'tp'=4] {'ep'}, dimensions={1} | all-to-all | bytes 2097152 | tf_op jit(solution)/shard_map/all_to_all | solution.py:97
  54.4 1.6 copy.40
  56.0 0.0 all-gather.3.cloned.1.call-update
  56.0 0.0 reduce-scatter.2.cloned.1.call-start
  56.0 33.6 %all-gather.3.cloned.1.call-done = bf16[128,8,2048]{2,1,0:T(8,128)(2,1)} async-done(((bf16[32,8,2048]{2,1,0:T(8,128)(2,1)}), bf16[128,8,2048]{2,1,0:T(8,128)(2,1)}) %all-gather.3.cloned.1.call-update) | async-done | bytes 4194320 | tf_op jit(solution)/shard_map/all_gather | solution.py:98
  89.7 6.6 %fusion.2 = f32[1024,512]{1,0:T(8,128)} fusion(bf16[128,8,2048]{2,1,0:T(8,128)(2,1)} %all-gather.3.cloned.1.call-done, bf16[1,2048,512]{2,1,0:T(8,128)(2,1)} %param.26), kind=kOutput, calls=%fused_computation.5 | convolution fusion | flops 2147483648 | bytes 8388608 | tf_op jit(solution)/shard_map/dot_general | solution.py:104
  96.2 0.0 copy-done
  96.2 10.3 %convolution_convert_fusion = bf16[1024,2048]{1,0:T(8,128)(2,1)} fusion(bf16[1,512,2048]{2,1,0:T(8,128)(2,1)S(1)} %copy-done, f32[1024,512]{1,0:T(8,128)} %fusion.2, bf16[1,2048,512]{2,1,0:T(8,128)(2,1)} %param.25, bf16[128,8,2048]{2,1,0:T(8,128)(2,1)} %all-gather.3.cloned.1.call-done), kind=kOutput, calls=%fused_computation.8 | convolution fusion | flops 4302307328 | bytes 14680064 | tf_op jit(solution)/shard_map/dot_general | solution.py:113
  106.5 0.0 reduce-scatter.2.cloned.1.call-update
  106.6 0.0 all-gather.5.cloned.1.call-start
  106.6 44.7 %reduce-scatter.2.cloned.1.call-done = bf16[256,2048]{1,0:T(8,128)(2,1)} async-done(((bf16[1024,2048]{1,0:T(8,128)(2,1)}), bf16[256,2048]{1,0:T(8,128)(2,1)}) %reduce-scatter.2.cloned.1.call-update) | async-done | bytes 1048592 | tf_op jit(solution)/shard_map/reduce_scatter | solution.py:112
  151.3 1.8 copy.41
  153.1 30.9 %all_to_all.11 = bf16[32,8,2048]{2,0,1:T(8,128)(2,1)S(1)} all-to-all(bf16[32,8,2048]{2,0,1:T(8,128)(2,1)S(1)} %copy.41), channel_id=1, replica_groups=mesh['ep'=8,'tp'=4] {'ep'}, dimensions={1} | all-to-all | bytes 2097152 | tf_op jit(solution)/shard_map/all_to_all | solution.py:118
  184.0 1.6 copy.42
  185.6 0.0 all-gather.5.cloned.1.call-update
  185.6 0.2 all-reduce.4.cloned.1.call-start
  185.9 0.0 copy-start.5
  185.9 0.2 convert_reduce_fusion.1
  186.0 0.3 fusion.27
  186.3 1.9 fusion.81
  188.2 0.0 copy-done.5
  188.3 0.0 copy-start.4
  188.3 0.0 copy-start.2
  188.3 0.0 copy-start.3
  188.3 0.0 copy-start.7
  188.3 0.5 fusion.23
  188.9 3.4 %collective-permute-start = (bf16[30,384]{1,0:T(8,128)(2,1)S(1)}, bf16[30,384]{1,0:T(8,128)(2,1)S(1)}, u32[]{:S(2)}, u32[]{:S(2)}) collective-permute-start(bf16[30,384]{1,0:T(8,128)(2,1)S(1)} %slice.260), channel_id=1, source_target_pairs={{0,4},{4,8},{8,12},{12,16},{16,20},{20,24},{24,28},{1,5},{5,9},{9,... | collective-permute-start | bytes 69128 | tf_op jit(solution)/shard_map/ppermute | solution.py:17
  192.2 0.1 mul.528
  192.4 0.1 copy.35
  192.5 0.1 slice_reduce_fusion.30
  192.5 0.1 slice_reduce_fusion.31
  192.6 0.0 copy-done.3
  192.7 0.1 copy.36
  192.8 0.1 copy.43
  192.9 0.8 collective-permute-done
  193.7 0.9 fusion.83
  194.7 6.5 %all-reduce.1 = (f32[128,1]{0,1:T(1,128)S(1)}, f32[128,1]{0,1:T(1,128)S(1)}) all-reduce(f32[128,1]{0,1:T(1,128)S(1)} %bitcast.51, f32[128,1]{0,1:T(1,128)S(1)} %bitcast.50), channel_id=1, replica_groups=mesh['ep'=8,'tp'=4] {'tp'}, use_global_device_ids=true, to_apply=%region_5.0 | all-reduce | flops 256 | bytes 2048 | tf_op jit(solution)/shard_map/psum | solution.py:56
  201.1 0.0 copy-done.7
  201.1 2.7 %convolution_convert_fusion.1 = bf16[128,2048]{1,0:T(8,128)(2,1)} fusion(bf16[384,2048]{1,0:T(8,128)(2,1)} %param.20, f32[128,384]{1,0:T(8,128)S(1)} %get-tuple-element.39, f32[384]{0:T(512)S(1)} %copy-done.7, f32[128]{0:T(128)S(1)} %get-tuple-element.41, f32[128]{0:T(128)S(1)} %get-tuple-element.40), kind=kOutput, calls=%fused_computation.9 | convolution fusion | flops 201981952 | bytes 2296320 | tf_op jit(solution)/shard_map/dot_general | solution.py:69
  203.9 0.0 all-reduce.4.cloned.1.call-update
  203.9 14.5 %all-gather.5.cloned.1.call-done = bf16[128,8,2048]{2,1,0:T(8,128)(2,1)} async-done(((bf16[32,8,2048]{2,1,0:T(8,128)(2,1)}), bf16[128,8,2048]{2,1,0:T(8,128)(2,1)}) %all-gather.5.cloned.1.call-update) | async-done | bytes 4194320 | tf_op jit(solution)/shard_map/all_gather | solution.py:121
  218.4 8.0 %gather_fusion.1 = bf16[512,2048]{1,0:T(8,128)(2,1)} fusion(bf16[1024,2048]{1,0:T(8,128)(2,1)} %bitcast.44, s32[1024]{0:T(1024)S(1)} %pad_clamp_fusion), kind=kCustom, calls=%fused_computation.1 | custom fusion | bytes 4196352 | tf_op jit(solution)/shard_map/jit(_take)/gather | solution.py:124
  226.4 4.1 %gather.15 = bf16[128,4,2048]{2,1,0:T(4,128)(2,1)} reshape(bf16[512,2048]{1,0:T(8,128)(2,1)} %gather_fusion.1) | data formatting | bytes 4194304 | tf_op jit(solution)/shard_map/jit(_take)/gather | solution.py:124
  230.6 6.4 %multiply_reduce_fusion = bf16[128,2048]{1,0:T(8,128)(2,1)} fusion(f32[128,4]{1,0:T(8,128)S(1)} %copy.43, bf16[128,4,2048]{2,1,0:T(4,128)(2,1)} %gather.15, pred[128,4]{1,0:T(8,128)(4,1)S(1)} %copy.36), kind=kLoop, calls=%fused_computation.7 | loop fusion | flops 3932160 | bytes 2624000 | tf_op jit(solution)/shard_map/reduce_sum | solution.py:126
  237.0 17.7 %all-reduce.4.cloned.1.call-done = bf16[128,2048]{1,0:T(8,128)(2,1)} async-done(((bf16[128,2048]{1,0:T(8,128)(2,1)}), bf16[128,2048]{1,0:T(8,128)(2,1)}) %all-reduce.4.cloned.1.call-update) | async-done | bytes 524304 | tf_op jit(solution)/shard_map/psum | solution.py:68
  254.7 1.9 copy.46
  (24 shorter events, 0.2 us)
Async XLA Ops:
  7.2 89.1 %copy-start = (bf16[1,512,2048]{2,1,0:T(8,128)(2,1)S(1)}, bf16[1,512,2048]{2,1,0:T(8,128)(2,1)}, u32[]{:S(2)}) copy-start(bf16[1,512,2048]{2,1,0:T(8,128)(2,1)} %param.27) | copy-start | bytes 6291460
  7.2 82.5 %all-gather.3.cloned.1.call-start = ((), (), s32[]{:S(2)}) async-start(), calls=%async_computation.4 | async-start | bytes 5242880 | tf_op jit(solution)/shard_map/all_gather | solution.py:98
  56.0 95.3 %reduce-scatter.2.cloned.1.call-start = ((), (), s32[]{:S(2)}) async-start(), calls=%async_computation.5 | async-start | bytes 5242880 | tf_op jit(solution)/shard_map/reduce_scatter | solution.py:112
  106.6 111.9 %all-gather.5.cloned.1.call-start = ((), (), s32[]{:S(2)}) async-start(), calls=%async_computation.6 | async-start | bytes 5242880 | tf_op jit(solution)/shard_map/all_gather | solution.py:121
  184.0 1.8 copy-start.1
  184.0 2.3 copy-start.6
  185.6 69.1 %all-reduce.4.cloned.1.call-start = ((), (), s32[]{:S(2)}) async-start(), calls=%async_computation.3 | async-start | bytes 1048576 | tf_op jit(solution)/shard_map/psum | solution.py:68
  185.9 2.4 copy-start.5
  188.3 4.2 %copy-start.4 = (f32[128,4]{0,1:T(4,128)S(1)}, f32[128,4]{0,1:T(4,128)}, u32[]{:S(2)}) copy-start(f32[128,4]{0,1:T(4,128)} %param.24) | copy-start | bytes 6148
  188.3 4.2 %copy-start.2 = (f32[31,384]{1,0:T(8,128)S(1)}, f32[31,384]{1,0:T(8,128)}, u32[]{:S(2)}) copy-start(f32[31,384]{1,0:T(8,128)} %param.18) | copy-start | bytes 142852
  188.3 4.4 %copy-start.3 = (s32[128,4]{0,1:T(4,128)S(1)}, s32[128,4]{0,1:T(4,128)}, u32[]{:S(2)}) copy-start(s32[128,4]{0,1:T(4,128)} %param.23) | copy-start | bytes 6148
  188.3 12.9 %copy-start.7 = (f32[384]{0:T(512)S(1)}, f32[384]{0:T(512)}, u32[]{:S(2)}) copy-start(f32[384]{0:T(512)} %param.19) | copy-start | bytes 4612
  188.9 4.9 %collective-permute-start = (bf16[30,384]{1,0:T(8,128)(2,1)S(1)}, bf16[30,384]{1,0:T(8,128)(2,1)S(1)}, u32[]{:S(2)}, u32[]{:S(2)}) collective-permute-start(bf16[30,384]{1,0:T(8,128)(2,1)S(1)} %slice.260), channel_id=1, source_target_pairs={{0,4},{4,8},{8,12},{12,16},{16,20},{20,24},{24,28},{1,5},{5,9},{9,... | collective-permute-start | bytes 69128 | tf_op jit(solution)/shard_map/ppermute | solution.py:17
Sparse Core Ops, SparseCore 0:
  56.1 33.4 all-gather.2
  106.7 44.5 reduce-scatter.1
  185.7 32.6 all-gather.4
  221.2 33.4 all-reduce.3
where the time goes:
time: 264 us; the launch traced here: 263 us
  waiting for transfers between devices  111 us (42%)
  blocking collectives  70.2 us (27%)
  local copies, waits for them, and re-layouts  26 us (10%)
  matrix products  22.1 us (8%)
  other arithmetic  15.7 us (6%)
  between operations  14 us (5%)
  starting transfers between devices  3.71 us (1%)
    reduce_scatter x1, waiting for transfers between devices, local(): lax.psum_scatter(jnp.dot(hidden, down_w, preferred_element_type=jnp.float...  44.7 us
    all_gather x1, waiting for transfers between devices, local(): block_rows = lax.all_gather(arrived, 'tp', axis=0, tiled=True)  33.6 us
    all_to_all x1, blocking collectives, local(): lax.all_to_all(sending, 'ep', split_axis=1, concat_axis=1, tiled=True)  32.8 us
    all_to_all x1, blocking collectives, local(): lax.all_to_all(summed.reshape(slot_share, experts, width), 'ep', split_ax...  30.9 us
    psum x1, waiting for transfers between devices, local(): lax.psum(jnp.dot(activated, w_output, preferred_element_type=jnp.float32)...  17.7 us
    all_gather x1, waiting for transfers between devices, local(): lax.all_gather(returned, 'tp', axis=0, tiled=True)  14.5 us
    gather x2, local copies, waits for them, and re-layouts, local(): picked = jnp.take(every_slot, slot_index * experts + flat_ids, axis=0)  12.1 us
    dot_general x1, matrix products, local(): jnp.dot(hidden, down_w, preferred_element_type=jnp.float32)  10.3 us
  transfers between devices with their start and end apart: 5, of which 5 were waited for; matrix products, arithmetic and copies ran while one was open for 10% of the time, Pallas kernels for 0%

commit v1 on v0

--- a/solution.py
+++ b/solution.py
@@ -65,8 +65,12 @@
     activated = jax.nn.silu(
         (conv_out - row_mean) * lax.rsqrt(row_var + epsilon) * channel_gain
     ).astype(jnp.bfloat16)
-    mixer_out = lax.psum(
-        jnp.dot(activated, w_output, preferred_element_type=jnp.float32).astype(jnp.bfloat16), "tp"
+    mixer_out = jnp.sum(
+        lax.all_gather(
+            jnp.dot(activated, w_output, preferred_element_type=jnp.float32).astype(jnp.bfloat16),
+            "tp",
+        ),
+        axis=0,
     )
     rows_b = expert_in.shape[0]
     width = expert_in.shape[1]

time: 264 us -> 244 us (0.924)
  waiting for transfers between devices: 111 us -> 90.2 us
  other arithmetic: 15.7 us -> 18.6 us
    reduce_scatter x1, waiting for transfers between devices: 44.7 us -> 26.2 us  [local(): lax.psum_scatter(jnp.dot(hidden, down_w, preferred_element_type=jnp.float...]
    psum x1 -> x0, waiting for transfers between devices: 17.7 us -> none  [local(): lax.psum(jnp.dot(activated, w_output, preferred_element_type=jnp.float32)...]
    all_gather x1, waiting for transfers between devices: 14.5 us -> 29.2 us  [local(): lax.all_gather(returned, 'tp', axis=0, tiled=True)]
    reduce_sum x0 -> x1, other arithmetic: none -> 2.92 us  [local(): jnp.sum(lax.all_gather(jnp.dot(activated, w_output, preferred_element_typ...]
  transfers between devices with their start and end apart: 5 -> 5, of which waited for: 5 -> 4; matrix products, arithmetic and copies ran while one was open for 10% -> 6% of each run, Pallas kernels for 0% -> 0%
where the time goes in v1:
time: 244 us; the launch traced here: 243 us
  waiting for transfers between devices  90.2 us (37%)
  blocking collectives  69.7 us (29%)
  local copies, waits for them, and re-layouts  25.1 us (10%)
  matrix products  22 us (9%)
  other arithmetic  18.6 us (8%)
  between operations  14 us (6%)
  starting transfers between devices  3.71 us (2%)
    all_gather x1, waiting for transfers between devices, local(): block_rows = lax.all_gather(arrived, 'tp', axis=0, tiled=True)  33.6 us
    all_to_all x1, blocking collectives, local(): lax.all_to_all(sending, 'ep', split_axis=1, concat_axis=1, tiled=True)  32.8 us
    all_to_all x1, blocking collectives, local(): lax.all_to_all(summed.reshape(slot_share, experts, width), 'ep', split_ax...  30.9 us
    all_gather x1, waiting for transfers between devices, local(): lax.all_gather(returned, 'tp', axis=0, tiled=True)  29.2 us
    reduce_scatter x1, waiting for transfers between devices, local(): lax.psum_scatter(jnp.dot(hidden, down_w, preferred_element_type=jnp.float...  26.2 us
    gather x2, local copies, waits for them, and re-layouts, local(): picked = jnp.take(every_slot, slot_index * experts + flat_ids, axis=0)  12.1 us
    dot_general x1, matrix products, local(): jnp.dot(hidden, down_w, preferred_element_type=jnp.float32)  10.3 us
    dot_general x1, matrix products, local(): jnp.dot(flat_rows, up_w, preferred_element_type=jnp.float32)  6.59 us
  transfers between devices with their start and end apart: 5, of which 4 were waited for; matrix products, arithmetic and copies ran while one was open for 6% of the time, Pallas kernels for 0%

profile of v1, /device:TPU:0, one launch (start us, length us, event | category | flops | bytes accessed | tf_op | source)
XLA Modules:
  0.0 243.4 jit_solution(6394160969569035820)
XLA Ops:
  7.2 0.0 copy-start
  7.2 0.0 all-gather.5.cloned.1.call-start
  7.2 0.9 copy.33
  8.2 0.1 eq.29
  8.3 0.1 eq.25
  8.4 0.1 reshape.119
  8.5 1.1 reduce-window.6
  9.7 0.2 slice_reduce_fusion
  9.9 0.1 fusion.68
  10.0 2.4 %scatter_custom_fusion = s32[1024]{0:T(1024)S(1)} fusion(s32[512]{0:T(512)S(1)} %bitcast.50, s32[512]{0:T(512)S(1)} %add_select_fusion, s32[]{:T(128)} %constant.84.clone.1), kind=kCustom, calls=%fused_computation.150 | custom fusion | bytes 4100 | tf_op jit(solution)/shard_map/scatter | solution.py:91
  12.5 0.1 compare_and_fusion
  12.6 1.2 convert_reduce_fusion
  13.8 1.3 fusion.24
  15.1 0.1 broadcast_in_dim.49
  15.2 0.1 copy.38
  15.3 1.4 fusion.26
  16.8 2.3 gather_fusion
  19.1 2.4 %copy_select_fusion = bf16[32,8,2048]{2,0,1:T(8,128)(2,1)S(1)} fusion(bf16[32,8,2048]{2,1,0:T(8,128)(2,1)} %bitcast.46, pred[32,8]{0,1:T(8,128)(4,1)S(1)} %copy.38), kind=kLoop, calls=%fused_computation.63 | loop fusion | flops 524288 | bytes 2097408 | tf_op jit(solution)/shard_map/jit(_take)/select_n | solution.py:100
  21.6 32.8 %all_to_all.10 = bf16[32,8,2048]{2,0,1:T(8,128)(2,1)S(1)} all-to-all(bf16[32,8,2048]{2,0,1:T(8,128)(2,1)S(1)} %copy_select_fusion), channel_id=1, replica_groups=mesh['ep'=8,'tp'=4] {'ep'}, dimensions={1} | all-to-all | bytes 2097152 | tf_op jit(solution)/shard_map/all_to_all | solution.py:101
  54.4 1.6 copy.40
  56.0 0.0 all-gather.5.cloned.1.call-update
  56.0 0.0 reduce-scatter.2.cloned.1.call-start
  56.1 33.6 %all-gather.5.cloned.1.call-done = bf16[128,8,2048]{2,1,0:T(8,128)(2,1)} async-done(((bf16[32,8,2048]{2,1,0:T(8,128)(2,1)}), bf16[128,8,2048]{2,1,0:T(8,128)(2,1)}) %all-gather.5.cloned.1.call-update) | async-done | bytes 4194320 | tf_op jit(solution)/shard_map/all_gather | solution.py:102
  89.7 6.6 %fusion.2 = f32[1024,512]{1,0:T(8,128)} fusion(bf16[128,8,2048]{2,1,0:T(8,128)(2,1)} %all-gather.5.cloned.1.call-done, bf16[1,2048,512]{2,1,0:T(8,128)(2,1)} %param.26), kind=kOutput, calls=%fused_computation.5 | convolution fusion | flops 2147483648 | bytes 8388608 | tf_op jit(solution)/shard_map/dot_general | solution.py:108
  96.3 0.0 copy-done
  96.3 10.3 %convolution_convert_fusion = bf16[1024,2048]{1,0:T(8,128)(2,1)} fusion(bf16[1,512,2048]{2,1,0:T(8,128)(2,1)S(1)} %copy-done, f32[1024,512]{1,0:T(8,128)} %fusion.2, bf16[1,2048,512]{2,1,0:T(8,128)(2,1)} %param.25, bf16[128,8,2048]{2,1,0:T(8,128)(2,1)} %all-gather.5.cloned.1.call-done), kind=kOutput, calls=%fused_computation.8 | convolution fusion | flops 4302307328 | bytes 14680064 | tf_op jit(solution)/shard_map/dot_general | solution.py:117
  106.5 0.0 reduce-scatter.2.cloned.1.call-update
  106.5 0.0 all-gather.9.cloned.1.call-start
  106.6 1.0 copy-done.1
  107.6 0.2 convert_reduce_fusion.1
  107.7 0.3 fusion.27
  108.0 0.0 copy-done.6
  108.0 1.9 fusion.81
  109.9 0.0 copy-done.5
  109.9 0.0 copy-start.2
  110.0 0.0 copy-start.7
  110.0 0.5 fusion.23
  110.5 3.5 %collective-permute-start = (bf16[30,384]{1,0:T(8,128)(2,1)S(1)}, bf16[30,384]{1,0:T(8,128)(2,1)S(1)}, u32[]{:S(2)}, u32[]{:S(2)}) collective-permute-start(bf16[30,384]{1,0:T(8,128)(2,1)S(1)} %slice.260), channel_id=1, source_target_pairs={{0,4},{4,8},{8,12},{12,16},{16,20},{20,24},{24,28},{1,5},{5,9},{9,... | collective-permute-start | bytes 69128 | tf_op jit(solution)/shard_map/ppermute | solution.py:17
  114.1 0.0 copy-done.2
  114.1 0.1 slice_reduce_fusion.31
  114.2 0.1 slice_reduce_fusion.30
  114.3 1.1 collective-permute-done
  115.4 0.9 fusion.83
  116.3 6.0 %all-reduce.1 = (f32[128,1]{0,1:T(1,128)S(1)}, f32[128,1]{0,1:T(1,128)S(1)}) all-reduce(f32[128,1]{0,1:T(1,128)S(1)} %bitcast.53, f32[128,1]{0,1:T(1,128)S(1)} %bitcast.52), channel_id=1, replica_groups=mesh['ep'=8,'tp'=4] {'tp'}, use_global_device_ids=true, to_apply=%region_5.0 | all-reduce | flops 256 | bytes 2048 | tf_op jit(solution)/shard_map/psum | solution.py:56
  122.3 0.0 copy-done.7
  122.3 2.7 %convolution_convert_fusion.1 = bf16[128,2048]{1,0:T(8,128)(2,1)} fusion(bf16[384,2048]{1,0:T(8,128)(2,1)} %param.20, f32[128,384]{1,0:T(8,128)S(1)} %get-tuple-element.39, f32[384]{0:T(512)S(1)} %copy-done.7, f32[128]{0:T(128)S(1)} %get-tuple-element.41, f32[128]{0:T(128)S(1)} %get-tuple-element.40), kind=kOutput, calls=%fused_computation.9 | convolution fusion | flops 201981952 | bytes 2296320 | tf_op jit(solution)/shard_map/dot_general | solution.py:70
  125.0 0.0 all-gather.9.cloned.1.call-update
  125.1 0.0 all-gather.7.cloned.1.call-start
  125.1 26.2 %reduce-scatter.2.cloned.1.call-done = bf16[256,2048]{1,0:T(8,128)(2,1)} async-done(((bf16[1024,2048]{1,0:T(8,128)(2,1)}), bf16[256,2048]{1,0:T(8,128)(2,1)}) %reduce-scatter.2.cloned.1.call-update) | async-done | bytes 1048592 | tf_op jit(solution)/shard_map/reduce_scatter | solution.py:116
  151.3 1.8 copy.41
  153.1 30.9 %all_to_all.11 = bf16[32,8,2048]{2,0,1:T(8,128)(2,1)S(1)} all-to-all(bf16[32,8,2048]{2,0,1:T(8,128)(2,1)S(1)} %copy.41), channel_id=1, replica_groups=mesh['ep'=8,'tp'=4] {'ep'}, dimensions={1} | all-to-all | bytes 2097152 | tf_op jit(solution)/shard_map/all_to_all | solution.py:122
  184.0 1.6 copy.42
  185.6 0.0 all-gather.7.cloned.1.call-update
  185.6 0.1 mul.528
  185.7 0.1 copy.35
  185.8 0.0 copy-done.3
  185.8 0.1 copy.36
  186.0 0.1 copy.43
  186.1 0.0 all-gather.9.cloned.1.call-done
  186.1 2.9 %reduce_sum.97 = bf16[128,2048]{1,0:T(8,128)(2,1)} reduce(bf16[4,128,2048]{2,1,0:T(8,128)(2,1)} %bitcast.47, bf16[]{:T(256)} %constant.78.clone.1), dimensions={0}, to_apply=%region_6.7 | reduce | flops 786432 | bytes 2621442 | tf_op jit(solution)/shard_map/reduce_sum | solution.py:68
  189.1 29.2 %all-gather.7.cloned.1.call-done = bf16[128,8,2048]{2,1,0:T(8,128)(2,1)} async-done(((bf16[32,8,2048]{2,1,0:T(8,128)(2,1)}), bf16[128,8,2048]{2,1,0:T(8,128)(2,1)}) %all-gather.7.cloned.1.call-update) | async-done | bytes 4194320 | tf_op jit(solution)/shard_map/all_gather | solution.py:125
  218.3 8.0 %gather_fusion.1 = bf16[512,2048]{1,0:T(8,128)(2,1)} fusion(bf16[1024,2048]{1,0:T(8,128)(2,1)} %bitcast.45, s32[1024]{0:T(1024)S(1)} %pad_clamp_fusion), kind=kCustom, calls=%fused_computation.1 | custom fusion | bytes 4196352 | tf_op jit(solution)/shard_map/jit(_take)/gather | solution.py:128
  226.3 4.1 %gather.15 = bf16[128,4,2048]{2,1,0:T(4,128)(2,1)} reshape(bf16[512,2048]{1,0:T(8,128)(2,1)} %gather_fusion.1) | data formatting | bytes 4194304 | tf_op jit(solution)/shard_map/jit(_take)/gather | solution.py:128
  230.4 6.4 %multiply_reduce_fusion = bf16[128,2048]{1,0:T(8,128)(2,1)} fusion(f32[128,4]{1,0:T(8,128)S(1)} %copy.43, bf16[128,4,2048]{2,1,0:T(4,128)(2,1)} %gather.15, pred[128,4]{1,0:T(8,128)(4,1)S(1)} %copy.36), kind=kLoop, calls=%fused_computation.7 | loop fusion | flops 3932160 | bytes 2624000 | tf_op jit(solution)/shard_map/reduce_sum | solution.py:130
  (24 shorter events, 0.2 us)
Async XLA Ops:
  7.2 89.1 %copy-start = (bf16[1,512,2048]{2,1,0:T(8,128)(2,1)S(1)}, bf16[1,512,2048]{2,1,0:T(8,128)(2,1)}, u32[]{:S(2)}) copy-start(bf16[1,512,2048]{2,1,0:T(8,128)(2,1)} %param.27) | copy-start | bytes 6291460
  7.2 82.5 %all-gather.5.cloned.1.call-start = ((), (), s32[]{:S(2)}) async-start(), calls=%async_computation.3 | async-start | bytes 5242880 | tf_op jit(solution)/shard_map/all_gather | solution.py:102
  56.0 95.2 %reduce-scatter.2.cloned.1.call-start = ((), (), s32[]{:S(2)}) async-start(), calls=%async_computation.4 | async-start | bytes 5242880 | tf_op jit(solution)/shard_map/reduce_scatter | solution.py:116
  106.5 1.0 copy-start.1
  106.5 1.5 copy-start.6
  106.5 79.6 %all-gather.9.cloned.1.call-start = ((), (), s32[]{:S(2)}) async-start(), calls=%async_computation.6 | async-start | bytes 2621440 | tf_op jit(solution)/shard_map/all_gather | solution.py:69
  107.6 2.4 copy-start.5
  109.9 4.1 %copy-start.2 = (f32[31,384]{1,0:T(8,128)S(1)}, f32[31,384]{1,0:T(8,128)}, u32[]{:S(2)}) copy-start(f32[31,384]{1,0:T(8,128)} %param.18) | copy-start | bytes 142852
  110.0 12.4 %copy-start.7 = (f32[384]{0:T(512)S(1)}, f32[384]{0:T(512)}, u32[]{:S(2)}) copy-start(f32[384]{0:T(512)} %param.19) | copy-start | bytes 4612
  110.5 4.9 %collective-permute-start = (bf16[30,384]{1,0:T(8,128)(2,1)S(1)}, bf16[30,384]{1,0:T(8,128)(2,1)S(1)}, u32[]{:S(2)}, u32[]{:S(2)}) collective-permute-start(bf16[30,384]{1,0:T(8,128)(2,1)S(1)} %slice.260), channel_id=1, source_target_pairs={{0,4},{4,8},{8,12},{12,16},{16,20},{20,24},{24,28},{1,5},{5,9},{9,... | collective-permute-start | bytes 69128 | tf_op jit(solution)/shard_map/ppermute | solution.py:17
  125.1 93.2 %all-gather.7.cloned.1.call-start = ((), (), s32[]{:S(2)}) async-start(), calls=%async_computation.5 | async-start | bytes 5242880 | tf_op jit(solution)/shard_map/all_gather | solution.py:125
  184.0 1.8 copy-start.3
  184.0 2.0 copy-start.4
Sparse Core Ops, SparseCore 0:
  56.1 33.4 all-gather.4
  106.7 44.5 reduce-scatter.1
  153.4 22.5 all-gather.8
  185.7 32.5 all-gather.6
